TPU v7x, 32 devices: a whole 2x2x4 slice. The times are simulated.
32 devices in a mesh: sp: 8 (over z, y), tp: 4 (over x, core).
Axes of the slice: x: 2, y: 2, z: 4, core: 2. Of those that a mesh axis runs over, the one named last changes fastest.
Arguments:
- queries: bfloat16 [4096, 1024], P('sp', 'tp'), may hold values from -200 to 200
- keys: bfloat16 [4096, 1024], P('sp', 'tp'), may hold values from -6 to 6
- values: bfloat16 [4096, 1024], P('sp', 'tp'), may hold values from -24 to 24
- cum_gate: float32 [4096, 8], P('sp', 'tp'), may hold values from -414 to 0, as said below
- residual: bfloat16 [4096, 2048], P(('sp', 'tp')), may hold values from -1.5 to 1.5
- w_out: bfloat16 [1024, 2048], replicated, may hold values from -0.1875 to 0.1875
- gain: float32 [2048], replicated, may hold values from 0.1 to 1.9
- w_up: bfloat16 [2048, 8192], P('sp', 'tp'), may hold values from -0.125 to 0.125
- w_down: bfloat16 [8192, 2048], P('tp', 'sp'), may hold values from -0.0625 to 0.0625
Outputs:
- output: bfloat16 [4096, 2048], P(('sp', 'tp'))
Inputs may be any that keep to these rules, and one draw needn't show every extreme that they name: Within each head, cum_gate never rises from one position to the next.
All inputs are finite; a program needn't handle non-finite values.
Results may differ from a plain program's by a relative error of at most 0.022.
Values may be sent and summed in bfloat16 or wider, within the bound.
A program may use at most 128 MiB of HBM per device.

v0:
```python
import math
import jax
import jax.numpy as jnp
from jax import lax
from jax.sharding import PartitionSpec as P


def per_device(queries, keys, values, cum_gate, residual, w_out, gain, w_up, w_down):
    tok_rows, width = queries.shape
    heads_here = cum_gate.shape[1]
    head_size = width // heads_here
    score_scale = head_size ** (-0.5)
    row_offset = lax.axis_index("sp") * tok_rows
    query_heads = queries.reshape(tok_rows, heads_here, head_size)
    query_pos = row_offset + jnp.arange(tok_rows, dtype=jnp.int32)
    all_gates = lax.all_gather(cum_gate, "sp", axis=0, tiled=True)
    initial = (
        jnp.full((tok_rows, heads_here), -1e30, jnp.float32),
        jnp.zeros((tok_rows, heads_here), jnp.float32),
        jnp.zeros((tok_rows, heads_here, head_size), jnp.float32),
    )
    carried = initial
    key_rows = lax.all_gather(keys, "sp", axis=0, tiled=True)
    value_rows = lax.all_gather(values, "sp", axis=0, tiled=True)
    row_count = key_rows.shape[0]
    span_rows = math.gcd(row_count, 2048)
    block_count = row_count // span_rows
    key_blocks = key_rows.reshape(block_count, span_rows, heads_here, head_size)
    value_blocks = value_rows.reshape(block_count, span_rows, heads_here, head_size)
    first_pos = jnp.arange(block_count, dtype=jnp.int32) * span_rows

    def absorb_block(running, packed):
        running_max, running_sum, accumulated = running
        key_blk, value_blk, block_start = packed
        gate_blk = lax.dynamic_slice_in_dim(all_gates, block_start, span_rows, 0)
        scores = jnp.einsum(
            "qhd,khd->qhk", query_heads, key_blk, preferred_element_type=jnp.float32
        )
        scores = scores * score_scale + cum_gate[:, :, None] - gate_blk.T[None, :, :]
        key_pos = block_start + jnp.arange(span_rows, dtype=jnp.int32)
        scores = jnp.where(key_pos[None, None, :] <= query_pos[:, None, None], scores, -1e30)
        new_max = jnp.maximum(running_max, jnp.max(scores, axis=-1))
        rescale = jnp.exp(running_max - new_max)
        weights = jnp.exp(scores - new_max[:, :, None])
        running_sum = running_sum * rescale + jnp.sum(weights, axis=-1)
        product = jnp.einsum(
            "qhk,khd->qhd",
            weights.astype(jnp.bfloat16),
            value_blk,
            preferred_element_type=jnp.float32,
        )
        accumulated = accumulated * rescale[:, :, None] + product
        return ((new_max, running_sum, accumulated), None)

    carried, _ = lax.scan(absorb_block, carried, (key_blocks, value_blocks, first_pos))
    running_max, running_sum, accumulated = carried
    attended = (accumulated / running_sum[:, :, None]).reshape(tok_rows, width).astype(jnp.bfloat16)
    mine = lax.all_to_all(attended, "tp", split_axis=0, concat_axis=1, tiled=True)
    projected = jnp.dot(mine, w_out, preferred_element_type=jnp.float32)
    residual_sum = residual.astype(jnp.float32) + projected
    mean_square = jnp.mean(residual_sum * residual_sum, axis=-1, keepdims=True)
    normed = (residual_sum * lax.rsqrt(mean_square + 1e-06) * gain).astype(jnp.bfloat16)
    normed_all = lax.all_gather(normed, "tp", axis=0, tiled=True)
    up_proj = jnp.dot(
        normed_all,
        lax.all_gather(w_up, "sp", axis=0, tiled=True),
        preferred_element_type=jnp.float32,
    )
    hidden = jnp.square(jax.nn.relu(up_proj)).astype(jnp.bfloat16)
    down_whole = lax.all_gather(w_down, "sp", axis=1, tiled=True)
    rounded = jnp.dot(hidden, down_whole, preferred_element_type=jnp.float32).astype(jnp.bfloat16)
    branch_out = lax.psum_scatter(
        lax.optimization_barrier(rounded).astype(jnp.float32).astype(jnp.bfloat16),
        "tp",
        scatter_dimension=0,
        tiled=True,
    ).astype(jnp.float32)
    return (residual_sum + branch_out).astype(jnp.bfloat16)


def solution(mesh):
    return jax.shard_map(
        per_device,
        mesh=mesh,
        in_specs=(
            P("sp", "tp"),
            P("sp", "tp"),
            P("sp", "tp"),
            P("sp", "tp"),
            P(("sp", "tp"), None),
            P(),
            P(),
            P("sp", "tp"),
            P("tp", "sp"),
        ),
        out_specs=P(("sp", "tp"), None),
        check_vma=False,
    )
```

profile of v0, /device:TPU:0, one launch (start us, length us, event | category | flops | bytes accessed | tf_op | source)
XLA Modules:
  0.0 501.9 jit_solution(15590965651173478988)
XLA Ops:
  6.5 0.0 copy-start
  6.5 0.0 all-gather.6.cloned.1.call-start
  6.5 0.7 all-gather.6.cloned.1.call-update
  7.3 0.0 all-gather.8.cloned.1.call-start
  7.3 0.7 all-gather.8.cloned.1.call-update
  8.0 0.0 all-gather.10.cloned.1.call-start
  8.1 1.1 copy.17
  9.2 0.2 copy.19
  9.4 32.7 %all_gather.19 = f32[4096,2]{0,1:T(2,128)S(1)} all-gather(f32[512,2]{0,1:T(2,128)} %param.14), channel_id=1, replica_groups=mesh['sp'=8,'tp'=4] {'sp'}, dimensions={0}, use_global_device_ids=true | all-gather | bytes 36864 | tf_op jit(solution)/shard_map/all_gather | solution.py:16
  42.0 19.4 %all-gather.6.cloned.1.call-done = bf16[4096,256]{1,0:T(8,128)(2,1)} async-done(((bf16[512,256]{1,0:T(8,128)(2,1)}), bf16[4096,256]{1,0:T(8,128)(2,1)}) %all-gather.6.cloned.1.call-update) | async-done | bytes 2097168 | tf_op jit(solution)/shard_map/all_gather | solution.py:23
  61.4 4.0 reshape.62
  65.4 45.8 %all-gather.8.cloned.1.call-done = bf16[4096,256]{1,0:T(8,128)(2,1)} async-done(((bf16[512,256]{1,0:T(8,128)(2,1)}), bf16[4096,256]{1,0:T(8,128)(2,1)}) %all-gather.8.cloned.1.call-update) | async-done | bytes 2097168 | tf_op jit(solution)/shard_map/all_gather | solution.py:24
  111.2 4.0 reshape.64
  115.2 0.0 copy-done
  115.2 45.9 %while.15 = (s32[]{:T(128)}, f32[512,2]{0,1:T(2,128)S(1)}, f32[512,2]{0,1:T(2,128)S(1)}, f32[512,2,128]{0,2,1:T(8,128)}, s32[2]{0:T(128)S(1)}, /*index=5*/bf16[2...) while((s32[]{:T(128)}, f32[512,2]{0,1:T(2,128)S(1)}, ...), condition=%wide.region_3.4_spmd.clone, body=%wide.region_0.3_spmd.clone.sunk | while | flops 1110842880 | bytes 39239884 | solution.py:55
  115.2 0.6 dynamic_slice.26
  117.4 0.1 dynamic-slice_bitcast_fusion.2
  117.5 0.6 iota_add_fusion.5
  118.1 0.8 broadcast_compare_fusion.2
  118.9 2.7 constant_dynamic-slice_fusion.3
  121.6 4.6 fusion.40
  126.2 4.8 fusion.42
  131.0 0.8 copy.34
  131.8 6.2 %fusion.44 = f32[512,2,128]{0,2,1:T(8,128)} fusion(f32[2,2048,512]{2,1,0:T(8,128)} %get-tuple-element.231, f32[512,2]{0,1:T(2,128)S(1)} %fusion.41, f32[2,2048]{1,0:T(2,128)S(1)} %dynamic-slice_bitcast_fusion.2, f32[512,2]{0,1:T(2,128)S(1)} %get-tuple-element.270, pred[512,2048]{0,1:T(8,128)(4,1)S(1)} %broadcast_compare_fusion.2, ...), kind=kOutput, calls=%fused_computation.12.clone.1 | convolution fusion | flops 549847040 | bytes 11563009 | tf_op jit(solution)/shard_map/while/body/eval_jaxpr/qhk,khd->qhd/dot_general | solution.py:46
  138.1 0.6 dynamic_slice.26
  140.3 0.1 dynamic-slice_bitcast_fusion.2
  140.4 0.6 iota_add_fusion.5
  141.0 0.8 broadcast_compare_fusion.2
  141.8 2.7 constant_dynamic-slice_fusion.3
  144.5 4.6 fusion.40
  149.1 4.8 fusion.42
  153.9 0.8 copy.34
  154.7 6.4 %fusion.44 = f32[512,2,128]{0,2,1:T(8,128)} fusion(f32[2,2048,512]{2,1,0:T(8,128)} %get-tuple-element.231, f32[512,2]{0,1:T(2,128)S(1)} %fusion.41, f32[2,2048]{1,0:T(2,128)S(1)} %dynamic-slice_bitcast_fusion.2, f32[512,2]{0,1:T(2,128)S(1)} %get-tuple-element.270, pred[512,2048]{0,1:T(8,128)(4,1)S(1)} %broadcast_compare_fusion.2, ...), kind=kOutput, calls=%fused_computation.12.clone.1 | convolution fusion | flops 549847040 | bytes 11563009 | tf_op jit(solution)/shard_map/while/body/eval_jaxpr/qhk,khd->qhd/dot_general | solution.py:46
  161.1 0.0 copy-start.1
  161.1 1.1 divide_convert_fusion
  162.2 0.1 reshape.65
  162.2 0.2 copy.24
  162.4 8.5 %all_to_all.16 = bf16[4,128,256]{2,1,0:T(8,128)(2,1)S(1)} all-to-all(bf16[4,128,256]{2,1,0:T(8,128)(2,1)S(1)} %copy.24), channel_id=1, replica_groups=mesh['sp'=8,'tp'=4] {'tp'}, dimensions={0} | all-to-all | bytes 524288 | tf_op jit(solution)/shard_map/all_to_all | solution.py:58
  171.0 0.2 copy.22
  171.1 3.1 multiply_reduce_fusion
  174.3 0.0 copy-done.1
  174.3 0.9 multiply_convert_fusion.1
  175.2 0.0 all-gather.10.cloned.1.call-update
  175.3 0.0 all-gather.12.cloned.1.call-start
  175.3 0.5 all-gather.12.cloned.1.call-update
  175.8 0.0 all-gather.14.cloned.1.call-start
  175.9 0.5 all-gather.14.cloned.1.call-update
  176.4 0.2 reduce-scatter.2.cloned.1.call-start
  176.7 19.0 %all-gather.10.cloned.1.call-done = bf16[512,2048]{1,0:T(8,128)(2,1)} async-done(((bf16[128,2048]{1,0:T(8,128)(2,1)}), bf16[512,2048]{1,0:T(8,128)(2,1)}) %all-gather.10.cloned.1.call-update) | async-done | bytes 2097168 | tf_op jit(solution)/shard_map/all_gather | solution.py:63
  195.6 126.5 %all-gather.12.cloned.1.call-done = bf16[2048,2048]{1,0:T(8,128)(2,1)} async-done(((bf16[256,2048]{1,0:T(8,128)(2,1)}), bf16[2048,2048]{1,0:T(8,128)(2,1)}) %all-gather.12.cloned.1.call-update) | async-done | bytes 8388624 | tf_op jit(solution)/shard_map/all_gather | solution.py:66
  322.1 125.0 %all-gather.14.cloned.1.call-done = bf16[2048,2048]{1,0:T(8,128)(2,1)} async-done(((bf16[2048,256]{1,0:T(8,128)(2,1)}), bf16[2048,2048]{1,0:T(8,128)(2,1)}) %all-gather.14.cloned.1.call-update) | async-done | bytes 8388624 | tf_op jit(solution)/shard_map/all_gather | solution.py:70
  447.1 16.5 %convolution_convert_fusion = bf16[512,2048]{1,0:T(8,128)(2,1)} fusion(bf16[2048,2048]{1,0:T(8,128)(2,1)} %all-gather.14.cloned.1.call-done, bf16[512,2048]{1,0:T(8,128)(2,1)} %all-gather.10.cloned.1.call-done, bf16[2048,2048]{1,0:T(8,128)(2,1)} %all-gather.12.cloned.1.call-done), kind=kOutput, calls=%fused_computation.30 | convolution fusion | flops 8594128896 | bytes 20971520 | tf_op jit(solution)/shard_map/dot_general | solution.py:71
  463.7 0.0 reduce-scatter.2.cloned.1.call-update
  463.7 29.5 %reduce-scatter.2.cloned.1.call-done = bf16[128,2048]{1,0:T(8,128)(2,1)} async-done(((bf16[512,2048]{1,0:T(8,128)(2,1)}), bf16[128,2048]{1,0:T(8,128)(2,1)}) %reduce-scatter.2.cloned.1.call-update) | async-done | bytes 524304 | tf_op jit(solution)/shard_map/reduce_scatter | solution.py:72
  493.2 1.9 add_convert_fusion
  (13 shorter events, 0.1 us)
Async XLA Ops:
  6.5 108.6 %copy-start = (f32[512,2]{0,1:T(2,128)S(1)}, f32[512,2]{0,1:T(2,128)}, u32[]{:S(2)}) copy-start(f32[512,2]{0,1:T(2,128)} %param.14) | copy-start | bytes 12292
  6.5 54.9 %all-gather.6.cloned.1.call-start = ((), (), s32[]{:S(2)}) async-start(), calls=%async_computation.2 | async-start | bytes 2359296 | tf_op jit(solution)/shard_map/all_gather | solution.py:23
  7.3 103.9 %all-gather.8.cloned.1.call-start = ((), (), s32[]{:S(2)}) async-start(), calls=%async_computation.3 | async-start | bytes 2359296 | tf_op jit(solution)/shard_map/all_gather | solution.py:24
  8.0 187.6 %all-gather.10.cloned.1.call-start = ((), (), s32[]{:S(2)}) async-start(), calls=%async_computation.4 | async-start | bytes 2621440 | tf_op jit(solution)/shard_map/all_gather | solution.py:63
  161.1 13.2 %copy-start.1 = (f32[2048]{0:T(1024)S(1)}, f32[2048]{0:T(1024)}, u32[]{:S(2)}) copy-start(f32[2048]{0:T(1024)} %param.17) | copy-start | bytes 24580
  175.3 146.8 %all-gather.12.cloned.1.call-start = ((), (), s32[]{:S(2)}) async-start(), calls=%async_computation.5 | async-start | bytes 9437184 | tf_op jit(solution)/shard_map/all_gather | solution.py:66
  175.8 271.3 %all-gather.14.cloned.1.call-start = ((), (), s32[]{:S(2)}) async-start(), calls=%async_computation.6 | async-start | bytes 9437184 | tf_op jit(solution)/shard_map/all_gather | solution.py:70
  176.4 316.7 %reduce-scatter.2.cloned.1.call-start = ((), (), s32[]{:S(2)}) async-start(), calls=%async_computation.7 | async-start | bytes 2621440 | tf_op jit(solution)/shard_map/reduce_scatter | solution.py:72
Sparse Core Ops, SparseCore 0:
  9.5 51.9 all-gather.5
  63.5 47.6 all-gather.7
  175.4 20.1 all-gather.9
  197.6 124.4 all-gather.11
  324.0 123.1 all-gather.13
  463.8 29.3 reduce-scatter.1
where the time goes:
time: 502 us
  waiting for transfers between devices  368 us (73%)
  matrix products  41.4 us (8%)
  blocking collectives  41.2 us (8%)
  local copies, waits for them, and re-layouts  18 us (4%)
  other arithmetic  16.3 us (3%)
  between operations  13.6 us (3%)
    all_gather x1, waiting for transfers between devices, per_device(): lax.all_gather(w_up, 'sp', axis=0, tiled=True)  126 us
    all_gather x1, waiting for transfers between devices, per_device(): down_whole = lax.all_gather(w_down, 'sp', axis=1, tiled=True)  125 us
    all_gather x1, waiting for transfers between devices, per_device(): value_rows = lax.all_gather(values, 'sp', axis=0, tiled=True)  45.8 us
    all_gather x1, blocking collectives, per_device(): all_gates = lax.all_gather(cum_gate, 'sp', axis=0, tiled=True)  32.7 us
    reduce_scatter x1, waiting for transfers between devices, per_device(): lax.psum_scatter(lax.optimization_barrier(rounded).astype(jnp.float32).as...  29.5 us
    all_gather x1, waiting for transfers between devices, per_device(): key_rows = lax.all_gather(keys, 'sp', axis=0, tiled=True)  19.4 us
    all_gather x1, waiting for transfers between devices, per_device(): normed_all = lax.all_gather(normed, 'tp', axis=0, tiled=True)  19 us
    dot_general x1, matrix products, per_device(): jnp.dot(hidden, down_whole, preferred_element_type=jnp.float32)  16.5 us
  transfers between devices with their start and end apart: 6, of which 6 were waited for; matrix products, arithmetic and copies ran while one was open for 1% of the time, Pallas kernels for 0%

commit v1 on v0

--- a/solution.py
+++ b/solution.py
@@ -67,7 +67,16 @@
         preferred_element_type=jnp.float32,
     )
     hidden = jnp.square(jax.nn.relu(up_proj)).astype(jnp.bfloat16)
-    down_whole = lax.all_gather(w_down, "sp", axis=1, tiled=True)
+    ndev = jax.lax.axis_size("sp")
+    all_blocks = [(kk, (kk + 1) % ndev) for kk in range(ndev)]
+    v_now = [None] * ndev
+    v_now[ndev - 1] = w_down
+    for u in range(ndev - 2, -1, -1):
+        v_now[u] = jax.lax.ppermute(v_now[u + 1], "sp", all_blocks)
+    x_now = jnp.concatenate(v_now, axis=1)
+    last = jax.lax.axis_index("sp")
+    p_next = (last + 1) * w_down.shape[1]
+    down_whole = jnp.roll(x_now, p_next, axis=1)
     rounded = jnp.dot(hidden, down_whole, preferred_element_type=jnp.float32).astype(jnp.bfloat16)
     branch_out = lax.psum_scatter(
         lax.optimization_barrier(rounded).astype(jnp.float32).astype(jnp.bfloat16),

time: 502 us -> 525 us (1.046)
  local copies, waits for them, and re-layouts: 18 us -> 47.1 us
  waiting for transfers between devices: 368 us -> 361 us
    ppermute x0 -> x7, waiting for transfers between devices: none -> 265 us  [per_device(): v_now[u] = jax.lax.ppermute(v_now[u + 1], 'sp', all_blocks)]
    all_gather x1, waiting for transfers between devices: 126 us -> 0.01 us  [per_device(): lax.all_gather(w_up, 'sp', axis=0, tiled=True)]
    all_gather x1 -> x0, waiting for transfers between devices: 125 us -> none  [per_device(): down_whole = lax.all_gather(w_down, 'sp', axis=1, tiled=True)]
    unnamed x6 -> x39, local copies, waits for them, and re-layouts: 1.27 us -> 29.2 us
    all_gather x1, waiting for transfers between devices: 19 us -> 0.01 us  [per_device(): normed_all = lax.all_gather(normed, 'tp', axis=0, tiled=True)]
  transfers between devices with their start and end apart: 6 -> 12, of which waited for: 6 -> 10; matrix products, arithmetic and copies ran while one was open for 1% -> 6% of each run, Pallas kernels for 0% -> 0%
where the time goes in v1:
time: 525 us
  waiting for transfers between devices  361 us (69%)
  local copies, waits for them, and re-layouts  47.1 us (9%)
  matrix products  41.6 us (8%)
  blocking collectives  41.2 us (8%)
  other arithmetic  16.4 us (3%)
  between operations  13.3 us (3%)
    ppermute x7, waiting for transfers between devices, per_device(): v_now[u] = jax.lax.ppermute(v_now[u + 1], 'sp', all_blocks)  265 us
    all_gather x1, waiting for transfers between devices, per_device(): value_rows = lax.all_gather(values, 'sp', axis=0, tiled=True)  45.7 us
    all_gather x1, blocking collectives, per_device(): all_gates = lax.all_gather(cum_gate, 'sp', axis=0, tiled=True)  32.7 us
    unnamed x39, local copies, waits for them, and re-layouts  29.2 us
    reduce_scatter x1, waiting for transfers between devices, per_device(): lax.psum_scatter(lax.optimization_barrier(rounded).astype(jnp.float32).as...  29 us
    all_gather x1, waiting for transfers between devices, per_device(): key_rows = lax.all_gather(keys, 'sp', axis=0, tiled=True)  19.4 us
    dot_general x1, matrix products, per_device(): jnp.dot(hidden, down_whole, preferred_element_type=jnp.float32)  16.5 us
    dot_general x2, matrix products, absorb_block(): jnp.einsum('qhk,khd->qhd', weights.astype(jnp.bfloat16), value_blk, prefe...  12.6 us
  transfers between devices with their start and end apart: 12, of which 10 were waited for; matrix products, arithmetic and copies ran while one was open for 6% of the time, Pallas kernels for 0%

profile of v1, /device:TPU:0, one launch (start us, length us, event | category | flops | bytes accessed | tf_op | source)
XLA Modules:
  0.0 524.7 jit_solution(5509641298809806234)
XLA Ops:
  6.5 0.7 all-gather.5.cloned.1.call-update
  7.3 0.7 all-gather.7.cloned.1.call-update
  8.1 1.1 copy.17
  9.2 0.2 copy.19
  9.4 32.7 %all_gather.16 = f32[4096,2]{0,1:T(2,128)S(1)} all-gather(f32[512,2]{0,1:T(2,128)} %param.14), channel_id=1, replica_groups=mesh['sp'=8,'tp'=4] {'sp'}, dimensions={0}, use_global_device_ids=true | all-gather | bytes 36864 | tf_op jit(solution)/shard_map/all_gather | solution.py:16
  42.0 19.4 %all-gather.5.cloned.1.call-done = bf16[4096,256]{1,0:T(8,128)(2,1)} async-done(((bf16[512,256]{1,0:T(8,128)(2,1)}), bf16[4096,256]{1,0:T(8,128)(2,1)}) %all-gather.5.cloned.1.call-update) | async-done | bytes 2097168 | tf_op jit(solution)/shard_map/all_gather | solution.py:23
  61.4 4.1 reshape.62
  65.5 45.7 %all-gather.7.cloned.1.call-done = bf16[4096,256]{1,0:T(8,128)(2,1)} async-done(((bf16[512,256]{1,0:T(8,128)(2,1)}), bf16[4096,256]{1,0:T(8,128)(2,1)}) %all-gather.7.cloned.1.call-update) | async-done | bytes 2097168 | tf_op jit(solution)/shard_map/all_gather | solution.py:24
  111.2 4.0 reshape.64
  115.2 46.1 %while.15 = (s32[]{:T(128)}, f32[512,2]{0,1:T(2,128)S(1)}, f32[512,2]{0,1:T(2,128)S(1)}, f32[512,2,128]{0,2,1:T(8,128)}, s32[2]{0:T(128)S(1)}, /*index=5*/bf16[2...) while((s32[]{:T(128)}, f32[512,2]{0,1:T(2,128)S(1)}, ...), condition=%wide.region_3.4_spmd.clone, body=%wide.region_0.3_spmd.clone.sunk | while | flops 1110842880 | bytes 39239884 | solution.py:55
  115.2 0.6 dynamic_slice.35
  117.6 0.6 iota_add_fusion.5
  118.2 0.8 broadcast_compare_fusion.2
  119.0 2.7 constant_dynamic-slice_fusion.3
  121.6 4.6 fusion.45
  126.3 4.8 fusion.47
  131.1 0.8 copy.34
  131.9 6.2 %fusion.49 = f32[512,2,128]{0,2,1:T(8,128)} fusion(f32[2,2048,512]{2,1,0:T(8,128)} %get-tuple-element.231, f32[512,2]{0,1:T(2,128)S(1)} %fusion.46, f32[2,2048]{1,0:T(2,128)S(1)} %dynamic-slice_bitcast_fusion.2, f32[512,2]{0,1:T(2,128)S(1)} %get-tuple-element.270, pred[512,2048]{0,1:T(8,128)(4,1)S(1)} %broadcast_compare_fusion.2, ...), kind=kOutput, calls=%fused_computation.12.clone.1 | convolution fusion | flops 549847040 | bytes 11563009 | tf_op jit(solution)/shard_map/while/body/eval_jaxpr/qhk,khd->qhd/dot_general | solution.py:46
  138.2 0.6 dynamic_slice.35
  140.6 0.6 iota_add_fusion.5
  141.2 0.8 broadcast_compare_fusion.2
  141.9 2.7 constant_dynamic-slice_fusion.3
  144.6 4.7 fusion.45
  149.3 4.8 fusion.47
  154.1 0.8 copy.34
  154.9 6.4 %fusion.49 = f32[512,2,128]{0,2,1:T(8,128)} fusion(f32[2,2048,512]{2,1,0:T(8,128)} %get-tuple-element.231, f32[512,2]{0,1:T(2,128)S(1)} %fusion.46, f32[2,2048]{1,0:T(2,128)S(1)} %dynamic-slice_bitcast_fusion.2, f32[512,2]{0,1:T(2,128)S(1)} %get-tuple-element.270, pred[512,2048]{0,1:T(8,128)(4,1)S(1)} %broadcast_compare_fusion.2, ...), kind=kOutput, calls=%fused_computation.12.clone.1 | convolution fusion | flops 549847040 | bytes 11563009 | tf_op jit(solution)/shard_map/while/body/eval_jaxpr/qhk,khd->qhd/dot_general | solution.py:46
  161.3 1.2 divide_convert_fusion
  162.5 0.2 copy.24
  162.7 8.5 %all_to_all.16 = bf16[4,128,256]{2,1,0:T(8,128)(2,1)S(1)} all-to-all(bf16[4,128,256]{2,1,0:T(8,128)(2,1)S(1)} %copy.24), channel_id=1, replica_groups=mesh['sp'=8,'tp'=4] {'tp'}, dimensions={0} | all-to-all | bytes 524288 | tf_op jit(solution)/shard_map/all_to_all | solution.py:58
  171.2 0.2 copy.22
  171.4 3.1 multiply_reduce_fusion
  174.6 0.9 multiply_convert_fusion.1
  175.6 0.5 all-gather.11.cloned.1.call-update
  176.2 0.6 collective-permute-start
  176.8 26.7 %collective-permute-done = bf16[2048,256]{1,0:T(8,128)(2,1)S(1)} collective-permute-done((bf16[2048,256]{1,0:T(8,128)(2,1)S(1)}, bf16[2048,256]{1,0:T(8,128)(2,1)S(1)}, u32[]{:S(2)}, u32[]{:S(2)}) %collective-permute-start) | collective-permute-done | bytes 1048608 | tf_op jit(solution)/shard_map/ppermute | solution.py:75
  203.5 46.6 %collective-permute-done.1 = bf16[2048,256]{1,0:T(8,128)(2,1)S(1)} collective-permute-done((bf16[2048,256]{1,0:T(8,128)(2,1)S(1)}, bf16[2048,256]{1,0:T(8,128)(2,1)S(1)}, u32[]{:S(2)}, u32[]{:S(2)}) %collective-permute-start.1) | collective-permute-done | bytes 1048608 | tf_op jit(solution)/shard_map/ppermute | solution.py:75
  250.0 1.0 copy-done.1
  251.1 41.5 %collective-permute-done.2 = bf16[2048,256]{1,0:T(8,128)(2,1)S(1)} collective-permute-done((bf16[2048,256]{1,0:T(8,128)(2,1)S(1)}, bf16[2048,256]{1,0:T(8,128)(2,1)S(1)}, u32[]{:S(2)}, u32[]{:S(2)}) %collective-permute-start.2) | collective-permute-done | bytes 1048608 | tf_op jit(solution)/shard_map/ppermute | solution.py:75
  292.6 1.0 copy-done.3
  293.6 49.1 %collective-permute-done.3 = bf16[2048,256]{1,0:T(8,128)(2,1)S(1)} collective-permute-done((bf16[2048,256]{1,0:T(8,128)(2,1)S(1)}, bf16[2048,256]{1,0:T(8,128)(2,1)S(1)}, u32[]{:S(2)}, u32[]{:S(2)}) %collective-permute-start.3) | collective-permute-done | bytes 1048608 | tf_op jit(solution)/shard_map/ppermute | solution.py:75
  342.7 1.0 copy-done.5
  343.7 49.1 %collective-permute-done.4 = bf16[2048,256]{1,0:T(8,128)(2,1)S(1)} collective-permute-done((bf16[2048,256]{1,0:T(8,128)(2,1)S(1)}, bf16[2048,256]{1,0:T(8,128)(2,1)S(1)}, u32[]{:S(2)}, u32[]{:S(2)}) %collective-permute-start.4) | collective-permute-done | bytes 1048608 | tf_op jit(solution)/shard_map/ppermute | solution.py:75
  392.7 1.0 copy-done.7
  393.7 27.3 %collective-permute-done.5 = bf16[2048,256]{1,0:T(8,128)(2,1)} collective-permute-done((bf16[2048,256]{1,0:T(8,128)(2,1)S(1)}, bf16[2048,256]{1,0:T(8,128)(2,1)}, u32[]{:S(2)}, u32[]{:S(2)}) %collective-permute-start.5) | collective-permute-done | bytes 1048608 | tf_op jit(solution)/shard_map/ppermute | solution.py:75
  421.0 24.7 %collective-permute-done.6 = bf16[2048,256]{1,0:T(8,128)(2,1)} collective-permute-done((bf16[2048,256]{1,0:T(8,128)(2,1)}, bf16[2048,256]{1,0:T(8,128)(2,1)}, u32[]{:S(2)}, u32[]{:S(2)}) %collective-permute-start.6) | collective-permute-done | bytes 1048608 | tf_op jit(solution)/shard_map/ppermute | solution.py:75
  445.7 2.3 constant_dynamic-update-slice_fusion.15
  448.1 2.3 constant_dynamic-update-slice_fusion.14
  450.4 2.4 constant_dynamic-update-slice_fusion.13
  452.8 2.4 constant_dynamic-update-slice_fusion.12
  455.2 1.1 constant_dynamic-update-slice_fusion.11
  456.3 1.1 constant_dynamic-update-slice_fusion.10
  457.4 1.1 constant_dynamic-update-slice_fusion.9
  458.5 1.1 constant_dynamic-update-slice_fusion.8
  459.6 2.3 constant_dynamic-update-slice_fusion.7
  461.9 2.3 constant_dynamic-update-slice_fusion.6
  464.2 1.1 constant_dynamic-update-slice_fusion.5
  465.3 1.1 constant_dynamic-update-slice_fusion.4
  466.4 1.1 constant_dynamic-update-slice_fusion.3
  467.5 1.1 constant_dynamic-update-slice_fusion.2
  468.6 1.1 constant_dynamic-update-slice_fusion.1
  469.7 1.1 constant_dynamic-update-slice_fusion
  470.8 16.5 %fusion.24 = bf16[512,2048]{1,0:T(8,128)(2,1)} fusion(bf16[2048,4096]{1,0:T(8,128)(2,1)} %constant_dynamic-update-slice_fusion, s32[]{:T(128)S(6)} %select_n.21, bf16[512,2048]{1,0:T(8,128)(2,1)} %all-gather.9.cloned.1.call-done, bf16[2048,2048]{1,0:T(8,128)(2,1)} %all-gather.11.cloned.1.call-done), kind=kOutput, calls=%fused_computation.32 | convolution fusion | flops 8594128896 | bytes 20971524 | tf_op jit(solution)/shard_map/dot_general | solution.py:80
  487.3 29.0 %reduce-scatter.2.cloned.1.call-done = bf16[128,2048]{1,0:T(8,128)(2,1)} async-done(((bf16[512,2048]{1,0:T(8,128)(2,1)}), bf16[128,2048]{1,0:T(8,128)(2,1)}) %reduce-scatter.2.cloned.1.call-update) | async-done | bytes 524304 | tf_op jit(solution)/shard_map/reduce_scatter | solution.py:81
  516.3 1.9 add_convert_fusion
  (49 shorter events, 0.6 us)
Async XLA Ops:
  6.5 108.7 %copy-start.9 = (f32[512,2]{0,1:T(2,128)S(1)}, f32[512,2]{0,1:T(2,128)}, u32[]{:S(2)}) copy-start(f32[512,2]{0,1:T(2,128)} %param.14) | copy-start | bytes 12292
  6.5 54.9 %all-gather.5.cloned.1.call-start = ((), (), s32[]{:S(2)}) async-start(), calls=%async_computation.2 | async-start | bytes 2359296 | tf_op jit(solution)/shard_map/all_gather | solution.py:23
  7.3 103.9 %all-gather.7.cloned.1.call-start = ((), (), s32[]{:S(2)}) async-start(), calls=%async_computation.3 | async-start | bytes 2359296 | tf_op jit(solution)/shard_map/all_gather | solution.py:24
  8.0 462.8 %all-gather.9.cloned.1.call-start = ((), (), s32[]{:S(2)}) async-start(), calls=%async_computation.4 | async-start | bytes 2621440 | tf_op jit(solution)/shard_map/all_gather | solution.py:63
  161.3 13.3 %copy-start.10 = (f32[2048]{0:T(1024)S(1)}, f32[2048]{0:T(1024)}, u32[]{:S(2)}) copy-start(f32[2048]{0:T(1024)} %param.17) | copy-start | bytes 24580
  161.3 14.9 %copy-start = (bf16[2048,256]{1,0:T(8,128)(2,1)S(1)}, bf16[2048,256]{1,0:T(8,128)(2,1)}, u32[]{:S(2)}) copy-start(bf16[2048,256]{1,0:T(8,128)(2,1)} %param.19) | copy-start | bytes 3145732
  175.5 295.2 %all-gather.11.cloned.1.call-start = ((), (), s32[]{:S(2)}) async-start(), calls=%async_computation.5 | async-start | bytes 9437184 | tf_op jit(solution)/shard_map/all_gather | solution.py:66
  176.1 340.1 %reduce-scatter.2.cloned.1.call-start = ((), (), s32[]{:S(2)}) async-start(), calls=%async_computation.6 | async-start | bytes 2621440 | tf_op jit(solution)/shard_map/reduce_scatter | solution.py:81
  176.2 27.3 %collective-permute-start = (bf16[2048,256]{1,0:T(8,128)(2,1)S(1)}, bf16[2048,256]{1,0:T(8,128)(2,1)S(1)}, u32[]{:S(2)}, u32[]{:S(2)}) collective-permute-start(bf16[2048,256]{1,0:T(8,128)(2,1)S(1)} %copy-done), channel_id=1, source_target_pairs={{0,4},{4,8},{8,12},{12,16},{16,20},{20,24},{24,28},{28,0},{1,5},{5... | collective-permute-start | bytes 3145736 | tf_op jit(solution)/shard_map/ppermute | solution.py:75
  203.5 46.6 %collective-permute-start.1 = (bf16[2048,256]{1,0:T(8,128)(2,1)S(1)}, bf16[2048,256]{1,0:T(8,128)(2,1)S(1)}, u32[]{:S(2)}, u32[]{:S(2)}) collective-permute-start(bf16[2048,256]{1,0:T(8,128)(2,1)S(1)} %collective-permute-done), channel_id=1, source_target_pairs={{0,4},{4,8},{8,12},{12,16},{16,20},{20,24},{24,28},{28,0},{1,5},{5... | collective-permute-start | bytes 3145736 | tf_op jit(solution)/shard_map/ppermute | solution.py:75
  250.0 1.0 copy-start.1
  251.1 41.5 %collective-permute-start.2 = (bf16[2048,256]{1,0:T(8,128)(2,1)S(1)}, bf16[2048,256]{1,0:T(8,128)(2,1)S(1)}, u32[]{:S(2)}, u32[]{:S(2)}) collective-permute-start(bf16[2048,256]{1,0:T(8,128)(2,1)S(1)} %collective-permute-done.1), channel_id=1, source_target_pairs={{0,4},{4,8},{8,12},{12,16},{16,20},{20,24},{24,28},{28,0},{1,5},{5... | collective-permute-start | bytes 3145736 | tf_op jit(solution)/shard_map/ppermute | solution.py:75
  292.6 1.0 copy-start.3
  293.6 49.1 %collective-permute-start.3 = (bf16[2048,256]{1,0:T(8,128)(2,1)S(1)}, bf16[2048,256]{1,0:T(8,128)(2,1)S(1)}, u32[]{:S(2)}, u32[]{:S(2)}) collective-permute-start(bf16[2048,256]{1,0:T(8,128)(2,1)S(1)} %collective-permute-done.2), channel_id=1, source_target_pairs={{0,4},{4,8},{8,12},{12,16},{16,20},{20,24},{24,28},{28,0},{1,5},{5... | collective-permute-start | bytes 3145736 | tf_op jit(solution)/shard_map/ppermute | solution.py:75
  342.7 1.0 copy-start.5
  343.7 49.1 %collective-permute-start.4 = (bf16[2048,256]{1,0:T(8,128)(2,1)S(1)}, bf16[2048,256]{1,0:T(8,128)(2,1)S(1)}, u32[]{:S(2)}, u32[]{:S(2)}) collective-permute-start(bf16[2048,256]{1,0:T(8,128)(2,1)S(1)} %collective-permute-done.3), channel_id=1, source_target_pairs={{0,4},{4,8},{8,12},{12,16},{16,20},{20,24},{24,28},{28,0},{1,5},{5... | collective-permute-start | bytes 3145736 | tf_op jit(solution)/shard_map/ppermute | solution.py:75
  392.7 1.0 copy-start.7
  393.7 27.3 %collective-permute-start.5 = (bf16[2048,256]{1,0:T(8,128)(2,1)S(1)}, bf16[2048,256]{1,0:T(8,128)(2,1)}, u32[]{:S(2)}, u32[]{:S(2)}) collective-permute-start(bf16[2048,256]{1,0:T(8,128)(2,1)S(1)} %collective-permute-done.4), channel_id=1, source_target_pairs={{0,4},{4,8},{8,12},{12,16},{16,20},{20,24},{24,28},{28,0},{1,5},{5... | collective-permute-start | bytes 3145736 | tf_op jit(solution)/shard_map/ppermute | solution.py:75
  421.0 24.7 %collective-permute-start.6 = (bf16[2048,256]{1,0:T(8,128)(2,1)}, bf16[2048,256]{1,0:T(8,128)(2,1)}, u32[]{:S(2)}, u32[]{:S(2)}) collective-permute-start(bf16[2048,256]{1,0:T(8,128)(2,1)} %collective-permute-done.5), channel_id=1, source_target_pairs={{0,4},{4,8},{8,12},{12,16},{16,20},{20,24},{24,28},{28,0},{1,5},{5... | collective-permute-start | bytes 3145736 | tf_op jit(solution)/shard_map/ppermute | solution.py:75
  421.0 34.1 %copy-start.4 = (bf16[2048,256]{1,0:T(8,128)(2,1)S(1)}, bf16[2048,256]{1,0:T(8,128)(2,1)}, u32[]{:S(2)}) copy-start(bf16[2048,256]{1,0:T(8,128)(2,1)} %copy-done.3) | copy-start | bytes 3145732
  421.0 35.2 %copy-start.2 = (bf16[2048,256]{1,0:T(8,128)(2,1)S(1)}, bf16[2048,256]{1,0:T(8,128)(2,1)}, u32[]{:S(2)}) copy-start(bf16[2048,256]{1,0:T(8,128)(2,1)} %copy-done.1) | copy-start | bytes 3145732
  450.4 13.8 %copy-start.8 = (bf16[2048,256]{1,0:T(8,128)(2,1)S(1)}, bf16[2048,256]{1,0:T(8,128)(2,1)}, u32[]{:S(2)}) copy-start(bf16[2048,256]{1,0:T(8,128)(2,1)} %copy-done.7) | copy-start | bytes 3145732
  452.8 12.5 %copy-start.6 = (bf16[2048,256]{1,0:T(8,128)(2,1)S(1)}, bf16[2048,256]{1,0:T(8,128)(2,1)}, u32[]{:S(2)}) copy-start(bf16[2048,256]{1,0:T(8,128)(2,1)} %copy-done.5) | copy-start | bytes 3145732
Sparse Core Ops, SparseCore 0:
  9.5 51.9 all-gather.4
  63.5 47.6 all-gather.6
  175.7 20.1 all-gather.8
  197.9 189.2 all-gather.10
  487.4 28.7 reduce-scatter.1
